TPU v7x, 256 devices: a 4x2x16 block of a 4x16x16 slice. The times are simulated.
256 devices in a mesh: grp: 2 (over y), sp: 32 (over z, core), tp: 4 (over x).
Axes of the slice: x: 4, y: 2, z: 16, core: 2. Of those that a mesh axis runs over, the one named last changes fastest.
The devices are a block of a 4x16x16 slice.
Arguments:
- residual: bfloat16 [16384, 2048], P(('grp', 'sp')), parts along dimension 0, may hold values from -6 to 6
- queries: bfloat16 [16384, 1024], P(('grp', 'sp'), 'tp'), parts along dimension 0, may hold values from -400 to 400
- keys: bfloat16 [16384, 1024], P(('grp', 'sp'), 'tp'), parts along dimension 0, may hold values from -8 to 8
- values: bfloat16 [16384, 1024], P(('grp', 'sp'), 'tp'), parts along dimension 0, may hold values from -6 to 6
- log_gates: float32 [16384, 16], P(('grp', 'sp'), 'tp'), parts along dimension 0, may hold values from -955 to 0, as said below
- w_out: bfloat16 [1024, 2048], P('tp'), may hold values from -0.75 to 0.75
- norm_gain: float32 [2048], replicated, may hold values from 0.1 to 1.9
- w_gate: bfloat16 [2048, 5632], P('sp', 'tp'), may hold values from -0.125 to 0.125
- w_up: bfloat16 [2048, 5632], P('sp', 'tp'), may hold values from -0.125 to 0.125
- w_down: bfloat16 [5632, 2048], P('tp', 'sp'), may hold values from -0.078125 to 0.078125
Outputs:
- output: bfloat16 [16384, 2048], P(('grp', 'sp', 'tp')), parts along dimension 0
There are 2 independent parts, one for each index of `grp`. A program takes and returns all parts, laid end to end along the dimension named above; an argument that names none is the same for every part. Nothing has to cross between parts.
Inputs may be any that keep to these rules, and one draw needn't show every extreme that they name: `log_gates`: never rises along positions.
All inputs are finite; a program needn't handle non-finite values.
Results may differ from a plain program's by a relative error of at most 0.014.
Values may be sent and summed in bfloat16 or wider, within the bound.
A program may use at most 128 MiB of HBM per device.

v0:
```python
import math
import jax
import jax.numpy as jnp
from jax import lax
from jax.sharding import PartitionSpec as P


def turned_gather(arrays, axis, dims):
    turned = [jnp.moveaxis(a, dim, 0) for a, dim in zip(arrays, dims)]
    widths = [t[0].size for t in turned]
    both = jnp.concatenate([t.reshape(-1, w) for t, w in zip(turned, widths)], axis=1)
    result = lax.all_gather(both, axis, axis=0, tiled=True)
    parts = jnp.split(result, [sum(widths[:k]) for k in range(1, len(widths))], axis=1)
    return tuple(
        (
            jnp.moveaxis(b.reshape(-1, *t.shape[1:]), 0, dim)
            for b, t, dim in zip(parts, turned, dims)
        )
    )


def cut_along(value, dim, peers):
    before, after = (value.shape[:dim], value.shape[dim + 1 :])
    return jnp.moveaxis(value.reshape(*before, peers, -1, *after), dim, 0)


def sent_and_summed(value, axis, dim):
    parts = cut_along(value, dim, lax.axis_size(axis))
    arrived = lax.all_to_all(parts, axis, split_axis=0, concat_axis=0, tiled=True)
    return arrived.astype(jnp.float32).sum(axis=0)


def sent_to_all(value, axis):
    copies = jnp.broadcast_to(value, (lax.axis_size(axis), *value.shape))
    return lax.all_to_all(copies, axis, split_axis=0, concat_axis=0, tiled=True)


def laid_out(parts, dim):
    parts = jnp.moveaxis(parts, 0, dim)
    dims = parts.shape
    return parts.reshape(*dims[:dim], dims[dim] * dims[dim + 1], *dims[dim + 2 :])


def gather_directly(value, axis, dim):
    parts = sent_to_all(value, axis)
    return laid_out(parts, dim)


def normalize(rows_in, gain):
    floats = rows_in.astype(jnp.float32)
    scaled = floats * lax.rsqrt(jnp.mean(floats * floats, axis=-1, keepdims=True) + 1e-06)
    return (scaled * gain).astype(jnp.bfloat16)


def attend(queries, keys, values, log_gates):
    row_count = queries.shape[0]
    head_count = log_gates.shape[1]
    head_width = queries.shape[1] // head_count
    score_scale = head_width ** (-0.5)
    first_row = lax.axis_index("sp") * row_count
    query_heads = queries.reshape(row_count, head_count, head_width)
    query_gates = log_gates.T
    query_positions = first_row + jnp.arange(row_count, dtype=jnp.int32)
    initial = (
        jnp.full((head_count, row_count), -1e30, jnp.float32),
        jnp.zeros((head_count, row_count), jnp.float32),
        jnp.zeros((head_count, row_count, head_width), jnp.float32),
    )
    carried = initial
    key_piece = lax.all_gather(keys.astype(jnp.float32), "sp", axis=0, tiled=True).astype(
        jnp.bfloat16
    )
    value_piece = lax.all_gather(values.astype(jnp.float32), "sp", axis=0, tiled=True).astype(
        jnp.bfloat16
    )
    gate_piece = lax.all_gather(log_gates, "sp", axis=0, tiled=True)
    length = key_piece.shape[0]
    block_rows = math.gcd(length, 2048)
    block_count = length // block_rows
    key_blocks = key_piece.reshape(block_count, block_rows, head_count, head_width)
    value_blocks = value_piece.reshape(block_count, block_rows, head_count, head_width)
    gate_blocks = gate_piece.reshape(block_count, block_rows, head_count)
    offsets = jnp.arange(block_count, dtype=jnp.int32) * block_rows

    def one_block(state, inputs):
        current_key_block, value_block, gate_block, offset = inputs

        def work(current):
            running_max, running_sum, accumulated = current
            scores = (
                jnp.einsum(
                    "qhd,khd->hqk",
                    query_heads,
                    current_key_block,
                    preferred_element_type=jnp.float32,
                )
                * score_scale
            )
            scores = scores + query_gates[:, :, None] - gate_block.T[:, None, :]
            key_positions = offset + jnp.arange(block_rows, dtype=jnp.int32)
            causal = (query_positions[:, None] >= key_positions[None, :])[None]
            scores = jnp.where(causal, scores, -1e30)
            new_max = jnp.maximum(running_max, jnp.max(scores, axis=-1))
            weights = jnp.where(causal, jnp.exp(scores - new_max[:, :, None]), 0.0)
            rescale = jnp.exp(running_max - new_max)
            running_sum = running_sum * rescale + jnp.sum(weights, axis=-1)
            product = jnp.einsum(
                "hqk,khd->hqd",
                weights.astype(jnp.bfloat16),
                value_block,
                preferred_element_type=jnp.float32,
            )
            accumulated = accumulated * rescale[:, :, None] + product
            return (new_max, running_sum, accumulated)

        state = lax.cond(offset <= first_row + row_count - 1, work, lambda current: current, state)
        return (state, None)

    carried, _ = lax.scan(one_block, carried, (key_blocks, value_blocks, gate_blocks, offsets))
    running_max, running_sum, accumulated = carried
    attended = accumulated / running_sum[:, :, None]
    return (
        attended.transpose(1, 0, 2).reshape(row_count, head_count * head_width).astype(jnp.bfloat16)
    )


def body(residual, queries, keys, values, log_gates, w_out, norm_gain, w_gate, w_up, w_down):
    gate_whole, up_whole, down_whole = turned_gather((w_gate, w_up, w_down), "sp", (0, 0, 1))
    attended = attend(queries, keys, values, log_gates)
    row_count = attended.shape[0]
    per_device = row_count // lax.axis_size("tp")
    my_first = lax.axis_index("tp") * per_device
    rows_part = attended
    projected = sent_and_summed(
        jnp.dot(rows_part, w_out, preferred_element_type=jnp.float32).astype(jnp.bfloat16), "tp", 0
    )
    own_rows = lax.dynamic_slice_in_dim(residual, my_first, per_device, 0)
    mixed = (own_rows.astype(jnp.float32) + projected).astype(jnp.bfloat16)
    normed_all = gather_directly(normalize(mixed, norm_gain), "tp", 0)
    gate_proj = jnp.dot(normed_all, gate_whole, preferred_element_type=jnp.float32)
    up_proj = jnp.dot(normed_all, up_whole, preferred_element_type=jnp.float32)
    hidden = (jax.nn.silu(gate_proj) * up_proj).astype(jnp.bfloat16)
    rows_part = hidden
    down_sum = sent_and_summed(
        jnp.dot(rows_part, down_whole, preferred_element_type=jnp.float32).astype(jnp.bfloat16),
        "tp",
        0,
    )
    summed = mixed.astype(jnp.float32) + 0.5 * down_sum
    scaled = summed * lax.rsqrt(jnp.mean(summed * summed, axis=-1, keepdims=True) + 1e-06)
    return scaled.astype(jnp.bfloat16)


def solution(mesh):
    in_specs = (
        P(("grp", "sp"), None),
        P(("grp", "sp"), "tp"),
        P(("grp", "sp"), "tp"),
        P(("grp", "sp"), "tp"),
        P(("grp", "sp"), "tp"),
        P("tp", None),
        P(),
        P("sp", "tp"),
        P("sp", "tp"),
        P("tp", "sp"),
    )
    out_specs = P(("grp", "sp", "tp"), None)
    return jax.shard_map(body, mesh=mesh, in_specs=in_specs, out_specs=out_specs, check_vma=False)
```

profile of v0, /device:TPU:33, one launch (start us, length us, event | category | flops | bytes accessed | tf_op | source)
XLA Modules:
  0.0 313.2 jit_solution(8759810375416187780)
XLA Ops:
  8.2 2.0 pad_maximum_fusion
  10.2 1.0 copy.15
  11.2 51.1 %all_gather.13 = f32[8192,4]{0,1:T(4,128)S(1)} all-gather(f32[256,4]{0,1:T(4,128)} %param.18), channel_id=1, replica_groups=mesh['grp'=2,'sp'=32,'tp'=4] {'sp'}, dimensions={0}, use_global_device_ids=true | all-gather | bytes 135168 | tf_op jit(solution)/shard_map/all_gather | solution.py:76
  62.3 33.5 %all-gather.4.cloned.1.call-done = bf16[8192,256]{1,0:T(8,128)(2,1)} async-done(((bf16[256,256]{1,0:T(8,128)(2,1)}), bf16[8192,256]{1,0:T(8,128)(2,1)}) %all-gather.4.cloned.1.call-update) | async-done | bytes 4194320 | tf_op jit(solution)/shard_map/all_gather | solution.py:70
  95.8 12.9 %reshape.83 = bf16[4,2048,4,64]{3,2,1,0:T(4,128)(2,1)} reshape(bf16[8192,256]{1,0:T(8,128)(2,1)} %all-gather.4.cloned.1.call-done) | data formatting | bytes 8388608 | tf_op jit(solution)/shard_map/reshape | solution.py:80
  108.7 12.9 %copy.17 = bf16[4,2048,4,64]{1,3,2,0:T(8,128)(2,1)} copy(bf16[4,2048,4,64]{3,2,1,0:T(4,128)(2,1)} %reshape.83) | data formatting | bytes 8388608
  121.6 45.0 %all-gather.6.cloned.1.call-done = bf16[8192,256]{1,0:T(8,128)(2,1)} async-done(((bf16[256,256]{1,0:T(8,128)(2,1)}), bf16[8192,256]{1,0:T(8,128)(2,1)}) %all-gather.6.cloned.1.call-update) | async-done | bytes 4194320 | tf_op jit(solution)/shard_map/all_gather | solution.py:73
  166.6 12.9 %reshape.84 = bf16[4,2048,4,64]{3,2,1,0:T(4,128)(2,1)} reshape(bf16[8192,256]{1,0:T(8,128)(2,1)} %all-gather.6.cloned.1.call-done) | data formatting | bytes 8388608 | tf_op jit(solution)/shard_map/reshape | solution.py:81
  179.5 13.0 %copy.18 = bf16[4,2048,4,64]{1,3,2,0:T(8,128)(2,1)} copy(bf16[4,2048,4,64]{3,2,1,0:T(4,128)(2,1)} %reshape.84) | data formatting | bytes 8388608
  192.5 18.0 %while.17 = (s32[]{:T(128)}, f32[4,256]{1,0:T(4,128)S(1)}, f32[4,256]{1,0:T(4,128)S(1)}, f32[4,256,64]{1,2,0:T(8,128)S(1)}, s32[4]{0:T(128)S(1)}, /*index=5*/s32...) while((s32[]{:T(128)}, f32[4,256]{1,0:T(4,128)S(1)}, ...), condition=%wide.region_5.6_spmd.clone, body=%wide.region_0.5_spmd.clone.sunk | while | flops 577376512 | bytes 30278972 | solution.py:119
  193.9 12.6 %conditional.3 = ((f32[4,256]{1,0:T(4,128)S(1)}, f32[4,256]{1,0:T(4,128)S(1)}, f32[4,256,64]{1,2,0:T(8,128)S(1)})) conditional(s32[]{:T(128)} %convert_element_type.112, (f32[4,256]{1,0:T(4,128)S(1)}, f32[4,256]{1,0:T(4,128)S(1)}, f32[4,256,64]{1,2,0:T(8,128)S(1)}) %tuple.48, (s32[]{:T(128)}, s32[]{:T(128)}, bf16[4,2048,4,64]{1,3,2,0:T(8,128)(2,1)}, ...), branch_computations={%region_1.1_spmd, %region_2.4_spmd} | conditional | flops 577376512 | bytes 30277676 | solution.py:116
  195.1 4.2 %fusion.4 = (f32[4,256]{1,0:T(4,128)S(1)}, f32[4,2048,256]{2,1,0:T(8,128)S(1)}) fusion(f32[4,2048]{1,0:T(4,128)S(1)} %dynamic-slice_bitcast_fusion, f32[4,256]{1,0:T(4,128)S(1)} %get-tuple-element.229, pred[256,2048]{0,1:T(8,128)(4,1)S(1)} %broadcast_compare_fusion, bf16[256,4,64]{0,2,1:T(8,128)(2,1)S(1)} %get-tuple-element.228, ...), kind=kOutput, calls=%fused_computation.5 | convolution fusion | flops 278920192 | bytes 10134016 | tf_op jit(solution)/shard_map/while/body/eval_jaxpr/cond/branch_1_fun/qhd,khd->hqk/dot_general | solution.py:91
  199.3 2.9 fusion.3
  202.3 4.2 %fusion.8 = f32[4,256,64]{1,2,0:T(8,128)S(1)} fusion(f32[4,2048,256]{2,1,0:T(8,128)S(1)} %get-tuple-element.328, f32[4,256]{1,0:T(4,128)S(1)} %max.4, f32[4,2048]{1,0:T(4,128)S(1)} %dynamic-slice_bitcast_fusion, f32[4,256]{1,0:T(4,128)S(1)} %get-tuple-element.229, pred[256,2048]{0,1:T(8,128)(4,1)S(1)} %broadcast_compare_fusion, ...), kind=kOutput, calls=%fused_computation.8 | convolution fusion | flops 283246592 | bytes 10531328 | tf_op jit(solution)/shard_map/while/body/eval_jaxpr/cond/branch_1_fun/hqk,khd->hqd/dot_general | solution.py:107
  210.6 1.4 convolution_convert_fusion
  212.1 3.7 %all-to-all-start = ((bf16[4,64,2048]{2,1,0:T(8,128)(2,1)}), bf16[4,64,2048]{2,1,0:T(8,128)(2,1)S(1)}, u32[]{:S(2)}, u32[]{:S(2)}) async-start(bf16[4,64,2048]{2,1,0:T(8,128)(2,1)} %bitcast.10), calls=%async_computation | async-start | bytes 2097152 | tf_op jit(solution)/shard_map/all_to_all | solution.py:29
  215.8 14.6 %all-to-all-done = bf16[4,64,2048]{2,1,0:T(8,128)(2,1)S(1)} async-done(((bf16[4,64,2048]{2,1,0:T(8,128)(2,1)}), bf16[4,64,2048]{2,1,0:T(8,128)(2,1)S(1)}, u32[]{:S(2)}, u32[]{:S(2)}) %all-to-all-start) | async-done | bytes 1048608 | tf_op jit(solution)/shard_map/all_to_all | solution.py:29
  230.5 1.1 fusion.44
  232.0 15.9 %all_to_all.15 = bf16[4,64,2048]{2,1,0:T(8,128)(2,1)S(1)} all-to-all(bf16[4,64,2048]{2,1,0:T(8,128)(2,1)S(1)} %broadcast_in_dim.51), channel_id=1, replica_groups=mesh['grp'=2,'sp'=32,'tp'=4] {'tp'}, dimensions={0} | all-to-all | bytes 2097152 | tf_op jit(solution)/shard_map/all_to_all | solution.py:35
  247.9 25.4 %all-gather.8.cloned.1.call-done = bf16[2048,4224]{1,0:T(8,128)(2,1)} async-done(((bf16[64,4224]{1,0:T(8,128)(2,1)}), bf16[2048,4224]{1,0:T(8,128)(2,1)}) %all-gather.8.cloned.1.call-update) | async-done | bytes 17301520 | tf_op jit(solution)/shard_map/all_gather | solution.py:12
  273.3 5.6 %fusion.25 = f32[256,1408]{1,0:T(8,128)} fusion(bf16[256,2048]{1,0:T(8,128)(2,1)S(1)} %bitcast.41, bf16[2048,4224]{1,0:T(8,128)(2,1)} %all-gather.8.cloned.1.call-done), kind=kOutput, calls=%fused_computation.29 | convolution fusion | flops 1476395008 | bytes 8257536 | tf_op jit(solution)/shard_map/dot_general | solution.py:140
  278.9 8.2 %fusion.33 = bf16[256,2048]{1,0:T(8,128)(2,1)S(1)} fusion(bf16[2048,4224]{1,0:T(8,128)(2,1)} %all-gather.8.cloned.1.call-done, bf16[256,2048]{1,0:T(8,128)(2,1)S(1)} %bitcast.42, f32[256,1408]{1,0:T(8,128)} %fusion.25), kind=kOutput, calls=%fused_computation.34 | convolution fusion | flops 2955476992 | bytes 15073280 | tf_op jit(solution)/shard_map/dot_general | solution.py:145
  287.0 18.4 %all_to_all.16 = bf16[4,64,2048]{2,1,0:T(8,128)(2,1)S(1)} all-to-all(bf16[4,64,2048]{2,1,0:T(8,128)(2,1)S(1)} %bitcast.43), channel_id=1, replica_groups=mesh['grp'=2,'sp'=32,'tp'=4] {'tp'}, dimensions={0} | all-to-all | bytes 2097152 | tf_op jit(solution)/shard_map/all_to_all | solution.py:29
  305.8 0.8 multiply_convert_fusion
  (42 shorter events, 6.3 us)
Async XLA Ops:
  6.5 204.1 %copy-start = (bf16[256,2048]{1,0:T(8,128)(2,1)S(1)}, bf16[256,2048]{1,0:T(8,128)(2,1)}, u32[]{:S(2)}) copy-start(bf16[256,2048]{1,0:T(8,128)(2,1)} %param.19) | copy-start | bytes 3145732
  6.6 89.2 %all-gather.4.cloned.1.call-start = ((), (), s32[]{:S(2)}) async-start(), calls=%async_computation.3 | async-start | bytes 4325376 | tf_op jit(solution)/shard_map/all_gather | solution.py:70
  7.3 159.3 %all-gather.6.cloned.1.call-start = ((), (), s32[]{:S(2)}) async-start(), calls=%async_computation.4 | async-start | bytes 4325376 | tf_op jit(solution)/shard_map/all_gather | solution.py:73
  8.1 265.2 %all-gather.8.cloned.1.call-start = ((), (), s32[]{:S(2)}) async-start(), calls=%async_computation.5 | async-start | bytes 17842176 | tf_op jit(solution)/shard_map/all_gather | solution.py:12
  179.5 13.0 %copy-start.1 = (f32[256,4]{0,1:T(4,128)S(1)}, f32[256,4]{0,1:T(4,128)}, u32[]{:S(2)}) copy-start(f32[256,4]{0,1:T(4,128)} %param.18) | copy-start | bytes 12292
  192.5 39.2 %copy-start.2 = (f32[2048]{0:T(1024)S(1)}, f32[2048]{0:T(1024)}, u32[]{:S(2)}) copy-start(f32[2048]{0:T(1024)} %param.20) | copy-start | bytes 24580
  212.1 18.3 %all-to-all-start = ((bf16[4,64,2048]{2,1,0:T(8,128)(2,1)}), bf16[4,64,2048]{2,1,0:T(8,128)(2,1)S(1)}, u32[]{:S(2)}, u32[]{:S(2)}) async-start(bf16[4,64,2048]{2,1,0:T(8,128)(2,1)} %bitcast.10), calls=%async_computation | async-start | bytes 2097152 | tf_op jit(solution)/shard_map/all_to_all | solution.py:29
Sparse Core Ops, SparseCore 0:
  9.2 86.5 all-gather.3
  97.6 68.9 all-gather.5
  168.4 104.8 all-gather.7
where the time goes:
time: 315 us; the launch traced here: 313 us
  waiting for transfers between devices  120 us (38%)
  blocking collectives  85.4 us (27%)
  local copies, waits for them, and re-layouts  55.5 us (18%)
  matrix products  23.6 us (7%)
  between operations  13.3 us (4%)
  other arithmetic  8.64 us (3%)
  starting transfers between devices  3.8 us (1%)
    all_gather x1, blocking collectives, attend(): gate_piece = lax.all_gather(log_gates, 'sp', axis=0, tiled=True)  51.1 us
    all_gather x1, waiting for transfers between devices, attend(): lax.all_gather(values.astype(jnp.float32), 'sp', axis=0, tiled=True)  45 us
    all_gather x1, waiting for transfers between devices, attend(): lax.all_gather(keys.astype(jnp.float32), 'sp', axis=0, tiled=True)  33.5 us
    unnamed x9, local copies, waits for them, and re-layouts  26.9 us
    all_gather x1, waiting for transfers between devices, turned_gather(): result = lax.all_gather(both, axis, axis=0, tiled=True)  25.4 us
    all_to_all x1, blocking collectives, sent_and_summed(): lax.all_to_all(parts, axis, split_axis=0, concat_axis=0, tiled=True)  18.4 us
    all_to_all x1, blocking collectives, sent_to_all(): return lax.all_to_all(copies, axis, split_axis=0, concat_axis=0, tiled=True)  15.9 us
    all_to_all x1, waiting for transfers between devices, sent_and_summed(): lax.all_to_all(parts, axis, split_axis=0, concat_axis=0, tiled=True)  14.6 us
  transfers between devices with their start and end apart: 4, of which 4 were waited for; matrix products, arithmetic and copies ran while one was open for 23% of the time, Pallas kernels for 0%

commit v1 on v0

--- a/solution.py
+++ b/solution.py
@@ -9,7 +9,10 @@
     turned = [jnp.moveaxis(a, dim, 0) for a, dim in zip(arrays, dims)]
     widths = [t[0].size for t in turned]
     both = jnp.concatenate([t.reshape(-1, w) for t, w in zip(turned, widths)], axis=1)
-    result = lax.all_gather(both, axis, axis=0, tiled=True)
+    size = lax.axis_size(axis)
+    pieces = jnp.stack([both for _ in range(size)])
+    pieces = lax.all_to_all(pieces, axis, split_axis=0, concat_axis=0)
+    result = jnp.concatenate(pieces, axis=0)
     parts = jnp.split(result, [sum(widths[:k]) for k in range(1, len(widths))], axis=1)
     return tuple(
         (

time: 315 us -> 1090 us (3.46)
  blocking collectives: 85.4 us -> 866 us
    all_to_all x1, blocking collectives: 15.9 us -> 797 us  [turned_gather(): pieces = lax.all_to_all(pieces, axis, split_axis=0, concat_axis=0)]
    all_gather x1 -> x0, waiting for transfers between devices: 25.4 us -> none  [turned_gather(): result = lax.all_gather(both, axis, axis=0, tiled=True)]
    all_to_all x0 -> x1, waiting for transfers between devices: none -> 13.6 us  [sent_to_all(): return lax.all_to_all(copies, axis, split_axis=0, concat_axis=0, tiled=True)]
    unnamed x9 -> x17, local copies, waits for them, and re-layouts: 26.9 us -> 32.5 us
  transfers between devices with their start and end apart: 4 -> 4, of which waited for: 4 -> 4; matrix products, arithmetic and copies ran while one was open for 23% -> 2% of each run, Pallas kernels for 0% -> 0%
where the time goes in v1:
time: 1090 us
  blocking collectives  866 us (79%)
  waiting for transfers between devices  111 us (10%)
  local copies, waits for them, and re-layouts  63.8 us (6%)
  matrix products  21.9 us (2%)
  between operations  13.6 us (1%)
    all_to_all x1, blocking collectives, turned_gather(): pieces = lax.all_to_all(pieces, axis, split_axis=0, concat_axis=0)  797 us
    all_gather x1, blocking collectives, attend(): gate_piece = lax.all_gather(log_gates, 'sp', axis=0, tiled=True)  51.1 us
    all_gather x1, waiting for transfers between devices, attend(): lax.all_gather(values.astype(jnp.float32), 'sp', axis=0, tiled=True)  45.4 us
    all_gather x1, waiting for transfers between devices, attend(): lax.all_gather(keys.astype(jnp.float32), 'sp', axis=0, tiled=True)  35.7 us
    unnamed x17, local copies, waits for them, and re-layouts  32.5 us
  transfers between devices with their start and end apart: 4, of which 4 were waited for; matrix products, arithmetic and copies ran while one was open for 2% of the time, Pallas kernels for 0%

profile of v1, /device:TPU:33, one launch (start us, length us, event | category | flops | bytes accessed | tf_op | source)
XLA Modules:
  0.0 1092.7 jit_solution(9073076486681802630)
XLA Ops:
  9.1 51.1 %all_gather.10 = f32[8192,4]{0,1:T(4,128)S(1)} all-gather(f32[256,4]{0,1:T(4,128)} %param.18), channel_id=1, replica_groups=mesh['grp'=2,'sp'=32,'tp'=4] {'sp'}, dimensions={0}, use_global_device_ids=true | all-gather | bytes 135168 | tf_op jit(solution)/shard_map/all_gather | solution.py:79
  60.3 35.7 %all-gather.3.cloned.1.call-done = bf16[8192,256]{1,0:T(8,128)(2,1)} async-done(((bf16[256,256]{1,0:T(8,128)(2,1)}), bf16[8192,256]{1,0:T(8,128)(2,1)}) %all-gather.3.cloned.1.call-update) | async-done | bytes 4194320 | tf_op jit(solution)/shard_map/all_gather | solution.py:73
  95.9 12.9 %reshape.89 = bf16[4,2048,4,64]{3,2,1,0:T(4,128)(2,1)} reshape(bf16[8192,256]{1,0:T(8,128)(2,1)} %all-gather.3.cloned.1.call-done) | data formatting | bytes 8388608 | tf_op jit(solution)/shard_map/reshape | solution.py:83
  108.9 12.8 %copy.17 = bf16[4,2048,4,64]{1,3,2,0:T(8,128)(2,1)} copy(bf16[4,2048,4,64]{3,2,1,0:T(4,128)(2,1)} %reshape.89) | data formatting | bytes 8388608
  121.6 45.4 %all-gather.5.cloned.1.call-done = bf16[8192,256]{1,0:T(8,128)(2,1)} async-done(((bf16[256,256]{1,0:T(8,128)(2,1)}), bf16[8192,256]{1,0:T(8,128)(2,1)}) %all-gather.5.cloned.1.call-update) | async-done | bytes 4194320 | tf_op jit(solution)/shard_map/all_gather | solution.py:76
  167.1 12.9 %reshape.90 = bf16[4,2048,4,64]{3,2,1,0:T(4,128)(2,1)} reshape(bf16[8192,256]{1,0:T(8,128)(2,1)} %all-gather.5.cloned.1.call-done) | data formatting | bytes 8388608 | tf_op jit(solution)/shard_map/reshape | solution.py:84
  180.0 12.7 %copy.18 = bf16[4,2048,4,64]{1,3,2,0:T(8,128)(2,1)} copy(bf16[4,2048,4,64]{3,2,1,0:T(4,128)(2,1)} %reshape.90) | data formatting | bytes 8388608
  192.8 17.2 %while.17 = (s32[]{:T(128)}, f32[4,256]{1,0:T(4,128)S(1)}, f32[4,256]{1,0:T(4,128)S(1)}, f32[4,256,64]{1,2,0:T(8,128)S(1)}, s32[4]{0:T(128)S(1)}, /*index=5*/s32...) while((s32[]{:T(128)}, f32[4,256]{1,0:T(4,128)S(1)}, ...), condition=%wide.region_5.6_spmd.clone, body=%wide.region_0.5_spmd.clone.sunk | while | flops 577376512 | bytes 30278980 | solution.py:122
  194.0 12.4 %conditional.3 = ((f32[4,256]{1,0:T(4,128)S(1)}, f32[4,256]{1,0:T(4,128)S(1)}, f32[4,256,64]{1,2,0:T(8,128)S(1)})) conditional(s32[]{:T(128)} %convert_element_type.112, (f32[4,256]{1,0:T(4,128)S(1)}, f32[4,256]{1,0:T(4,128)S(1)}, f32[4,256,64]{1,2,0:T(8,128)S(1)}) %tuple.48, (s32[]{:T(128)}, s32[]{:T(128)}, bf16[4,2048,4,64]{1,3,2,0:T(8,128)(2,1)}, ...), branch_computations={%region_1.1_spmd, %region_2.4_spmd} | conditional | flops 577376512 | bytes 30277676 | solution.py:119
  195.1 4.2 fusion.4
  199.2 2.9 fusion.3
  202.2 4.2 fusion.8
  210.0 1.4 convolution_convert_fusion
  211.5 3.9 all-to-all-start
  215.3 14.6 %all-to-all-done = bf16[4,64,2048]{2,1,0:T(8,128)(2,1)S(1)} async-done(((bf16[4,64,2048]{2,1,0:T(8,128)(2,1)}), bf16[4,64,2048]{2,1,0:T(8,128)(2,1)S(1)}, u32[]{:S(2)}, u32[]{:S(2)}) %all-to-all-start) | async-done | bytes 1048608 | tf_op jit(solution)/shard_map/all_to_all | solution.py:32
  230.1 1.1 fusion.44
  232.5 3.6 all-to-all-start.1
  236.2 13.6 %all-to-all-done.1 = bf16[4,64,2048]{2,1,0:T(8,128)(2,1)S(1)} async-done(((bf16[4,64,2048]{2,1,0:T(8,128)(2,1)}), bf16[4,64,2048]{2,1,0:T(8,128)(2,1)S(1)}, u32[]{:S(2)}, u32[]{:S(2)}) %all-to-all-start.1) | async-done | bytes 1048608 | tf_op jit(solution)/shard_map/all_to_all | solution.py:38
  249.8 2.1 stack.2
  251.9 796.6 %all_to_all.20 = bf16[32,64,4224]{2,1,0:T(8,128)(2,1)S(1)} all-to-all(bf16[32,64,4224]{2,1,0:T(8,128)(2,1)S(1)} %stack.2), channel_id=1, replica_groups=mesh['grp'=2,'sp'=32,'tp'=4] {'sp'}, dimensions={0} | all-to-all | bytes 34603008 | tf_op jit(solution)/shard_map/all_to_all | solution.py:14
  1048.4 5.9 copy-done.1
  1054.3 3.0 fusion.25
  1057.3 9.2 fusion.33
  1066.5 18.2 %all_to_all.21 = bf16[4,64,2048]{2,1,0:T(8,128)(2,1)S(1)} all-to-all(bf16[4,64,2048]{2,1,0:T(8,128)(2,1)} %bitcast.46), channel_id=1, replica_groups=mesh['grp'=2,'sp'=32,'tp'=4] {'tp'}, dimensions={0} | all-to-all | bytes 2097152 | tf_op jit(solution)/shard_map/all_to_all | solution.py:32
  (50 shorter events, 8.7 us)
Async XLA Ops:
  6.5 203.5 %copy-start = (bf16[256,2048]{1,0:T(8,128)(2,1)S(1)}, bf16[256,2048]{1,0:T(8,128)(2,1)}, u32[]{:S(2)}) copy-start(bf16[256,2048]{1,0:T(8,128)(2,1)} %param.19) | copy-start | bytes 3145732
  6.6 89.4 %all-gather.3.cloned.1.call-start = ((), (), s32[]{:S(2)}) async-start(), calls=%async_computation.4 | async-start | bytes 4325376 | tf_op jit(solution)/shard_map/all_gather | solution.py:73
  7.3 159.8 %all-gather.5.cloned.1.call-start = ((), (), s32[]{:S(2)}) async-start(), calls=%async_computation.5 | async-start | bytes 4325376 | tf_op jit(solution)/shard_map/all_gather | solution.py:76
  180.0 12.8 %copy-start.5 = (f32[256,4]{0,1:T(4,128)S(1)}, f32[256,4]{0,1:T(4,128)}, u32[]{:S(2)}) copy-start(f32[256,4]{0,1:T(4,128)} %param.18) | copy-start | bytes 12292
  192.8 38.5 %copy-start.6 = (f32[2048]{0:T(1024)S(1)}, f32[2048]{0:T(1024)}, u32[]{:S(2)}) copy-start(f32[2048]{0:T(1024)} %param.20) | copy-start | bytes 24580
  209.9 26.2 %copy-start.2 = (bf16[1408,64]{0,1:T(8,128)(2,1)S(1)}, bf16[1408,64]{0,1:T(8,128)(2,1)}, u32[]{:S(2)}) copy-start(bf16[1408,64]{0,1:T(8,128)(2,1)} %param.23) | copy-start | bytes 540676
  210.0 26.2 %copy-start.3 = (bf16[64,1408]{1,0:T(8,128)(2,1)S(1)}, bf16[64,1408]{1,0:T(8,128)(2,1)}, u32[]{:S(2)}) copy-start(bf16[64,1408]{1,0:T(8,128)(2,1)} %param.22) | copy-start | bytes 540676
  210.0 26.2 %copy-start.4 = (bf16[64,1408]{1,0:T(8,128)(2,1)S(1)}, bf16[64,1408]{1,0:T(8,128)(2,1)}, u32[]{:S(2)}) copy-start(bf16[64,1408]{1,0:T(8,128)(2,1)} %param.21) | copy-start | bytes 540676
  211.5 18.5 %all-to-all-start = ((bf16[4,64,2048]{2,1,0:T(8,128)(2,1)}), bf16[4,64,2048]{2,1,0:T(8,128)(2,1)S(1)}, u32[]{:S(2)}, u32[]{:S(2)}) async-start(bf16[4,64,2048]{2,1,0:T(8,128)(2,1)} %bitcast.10), calls=%async_computation | async-start | bytes 2097152 | tf_op jit(solution)/shard_map/all_to_all | solution.py:32
  232.5 17.3 %all-to-all-start.1 = ((bf16[4,64,2048]{2,1,0:T(8,128)(2,1)}), bf16[4,64,2048]{2,1,0:T(8,128)(2,1)S(1)}, u32[]{:S(2)}, u32[]{:S(2)}) async-start(bf16[4,64,2048]{2,1,0:T(8,128)(2,1)} %broadcast_in_dim.51), calls=%async_computation.1 | async-start | bytes 2097152 | tf_op jit(solution)/shard_map/all_to_all | solution.py:38
  1048.4 5.9 copy-start.1
Sparse Core Ops, SparseCore 0:
  9.2 86.6 all-gather.2
  97.8 69.2 all-gather.4
